TPU v7x, 32 devices: a whole 2x2x4 slice. The times are simulated.
32 devices in a mesh: grp: 1, ep: 16 (over z, y, x), tp: 2 (over core).
Axes of the slice: x: 2, y: 2, z: 4, core: 2. Of those that a mesh axis runs over, the one named last changes fastest.
Arguments:
- tokens_in: bfloat16 [1024, 2048], P(('grp', 'ep')), may hold values from -6 to 6
- norm_gain: float32 [2048], replicated, may hold values from 0.1 to 1.9
- gate_proj: bfloat16 [16, 2048, 1024], P('ep', None, 'tp'), may hold values from -0.125 to 0.125
- up_proj: bfloat16 [16, 2048, 1024], P('ep', None, 'tp'), may hold values from -0.125 to 0.125
- down_proj: bfloat16 [16, 1024, 2048], P('ep', 'tp'), may hold values from -0.1875 to 0.1875
- route_ids: int32 [1024, 8], P(('grp', 'ep')), may hold values from 0 to 15, all different within a row; in each aligned block of 64 rows (0 to 63, 64 to 127, ...) at most 64 rows name the same one
- group_weight: float32 [1024, 2], P(('grp', 'ep')), may hold values from 0.05 to 1
- expert_weight: float32 [1024, 8], P(('grp', 'ep')), may hold values from 0.05 to 1
Outputs:
- expert_mix: bfloat16 [1024, 2048], P(('grp', 'ep'), 'tp')
Inputs may be any that keep to these rules, and one draw needn't show every extreme that they name: `route_ids`: each row names 8 different experts; within the rows of one index of ep no expert is named by more than 64 rows, a bound that some of them reach.
All inputs are finite; a program needn't handle non-finite values.
Results may differ from a plain program's by a relative error of at most 0.0077.
Values may be sent and summed in bfloat16 or wider, within the bound.
A program may use at most 64 MiB of HBM per device.

v0:
```python
import jax
import jax.numpy as jnp
from jax import lax
from jax.sharding import PartitionSpec as P

EXP_GRP = 8
EPSILON = 1e-06


def on_device(
    tokens_in, norm_gain, gate_proj, up_proj, down_proj, route_ids, group_weight, expert_weight
):
    token_count, model_width = tokens_in.shape
    expert_count = gate_proj.shape[0] * lax.axis_size("ep")
    lane_count = lax.axis_size("tp")
    lane_index = lax.axis_index("tp")
    share = token_count // lane_count
    own_rows = lax.dynamic_slice_in_dim(tokens_in, lane_index * share, share, 0)
    row_values = own_rows.astype(jnp.float32)
    inv_scale = lax.rsqrt(jnp.mean(row_values * row_values, axis=-1, keepdims=True) + EPSILON)
    normed = (row_values * inv_scale * norm_gain).astype(jnp.bfloat16)
    rows = lax.all_gather(normed, ("ep", "tp"), axis=0, tiled=True)
    experts = jnp.arange(expert_count, dtype=jnp.int32)
    share_of = expert_weight / jnp.sum(expert_weight, axis=1, keepdims=True)
    named = route_ids[:, :, None] == experts[None, None, :]
    chosen = jnp.sum(jnp.where(named, share_of[:, :, None], 0.0), axis=1)
    gates = chosen * jnp.repeat(group_weight, EXP_GRP, axis=1)
    all_gates = lax.all_gather(gates, "ep", axis=0, tiled=True)
    own_gate = lax.dynamic_slice_in_dim(all_gates, lax.axis_index("ep"), 1, 1)
    gate_acts = jnp.dot(rows, gate_proj[0], preferred_element_type=jnp.float32)
    up_acts = jnp.dot(rows, up_proj[0], preferred_element_type=jnp.float32)
    hidden = (jax.nn.silu(gate_acts) * up_acts).astype(jnp.bfloat16)
    partial_rows = jnp.dot(hidden, down_proj[0], preferred_element_type=jnp.float32)
    weighted = (partial_rows * own_gate).astype(jnp.bfloat16)
    halves = lax.psum_scatter(weighted, "tp", scatter_dimension=1, tiled=True)
    return lax.psum_scatter(halves, "ep", scatter_dimension=0, tiled=True)


def solution(mesh):
    in_specs = (
        P(("grp", "ep"), None),
        P(),
        P("ep", None, "tp"),
        P("ep", None, "tp"),
        P("ep", "tp", None),
        P(("grp", "ep"), None),
        P(("grp", "ep"), None),
        P(("grp", "ep"), None),
    )
    out_specs = P(("grp", "ep"), "tp")
    return jax.shard_map(
        on_device, mesh=mesh, in_specs=in_specs, out_specs=out_specs, check_vma=False
    )
```

profile of v0, /device:TPU:0, one launch (start us, length us, event | category | flops | bytes accessed | tf_op | source)
XLA Modules:
  0.0 194.1 jit_solution(4281065118066478844)
XLA Ops:
  6.5 0.0 copy-start
  6.5 0.0 all-gather.3.cloned.1.call-start
  6.5 1.2 fusion.9
  7.7 1.7 fusion.11
  9.4 0.0 all-gather.3.cloned.1.call-update
  9.4 0.0 reduce-scatter.3.cloned.1.call-start
  9.5 0.7 reduce_sum.28
  10.2 0.7 broadcast_divide_fusion
  10.9 0.7 select_reduce_fusion
  11.6 0.7 fusion.12
  12.3 43.3 %all-gather = f32[16,64,16]{1,2,0:T(8,128)S(1)} all-gather(f32[1,64,16]{1,2,0:T(8,128)S(1)} %fusion.12), channel_id=1, replica_groups=mesh['grp'=1,'ep'=16,'tp'=2] {'ep'}, dimensions={0}, use_global_device_ids=true | all-gather | bytes 69632 | tf_op jit(solution)/shard_map/all_gather | solution.py:28
  55.7 0.1 reshape.17
  55.8 19.2 %all-gather.3.cloned.1.call-done = bf16[1024,2048]{1,0:T(8,128)(2,1)} async-done(((bf16[32,2048]{1,0:T(8,128)(2,1)}), bf16[1024,2048]{1,0:T(8,128)(2,1)}) %all-gather.3.cloned.1.call-update) | async-done | bytes 4194320 | tf_op jit(solution)/shard_map/all_gather | solution.py:22
  75.0 6.6 %fusion.1 = f32[1024,512]{1,0:T(8,128)} fusion(bf16[1024,2048]{1,0:T(8,128)(2,1)} %all-gather.3.cloned.1.call-done, bf16[1,2048,512]{2,1,0:T(8,128)(2,1)} %param.11), kind=kOutput, calls=%fused_computation.2 | convolution fusion | flops 2147483648 | bytes 8388608 | tf_op jit(solution)/shard_map/dot_general | solution.py:31
  81.5 0.0 copy-done
  81.5 10.1 %multiply_convert_fusion = bf16[1024,2048]{1,0:T(8,128)(2,1)} fusion(f32[1024]{0:T(1024)S(1)} %bitcast.24, bf16[1,512,2048]{2,1,0:T(8,128)(2,1)S(1)} %copy-done, f32[1024,512]{1,0:T(8,128)} %fusion.1, bf16[1024,2048]{1,0:T(8,128)(2,1)} %all-gather.3.cloned.1.call-done, bf16[1,2048,512]{2,1,0:T(8,128)(2,1)} %param.10), kind=kOutput, calls=%fused_computation | convolution fusion | flops 4302307328 | bytes 14684160 | tf_op jit(solution)/shard_map/dot_general | solution.py:33
  91.6 0.0 reduce-scatter.3.cloned.1.call-update
  91.6 0.0 reduce-scatter.5.cloned.1.call-start
  91.7 10.8 %reduce-scatter.3.cloned.1.call-done = bf16[1024,1024]{1,0:T(8,128)(2,1)} async-done(((bf16[1024,2048]{1,0:T(8,128)(2,1)}), bf16[1024,1024]{1,0:T(8,128)(2,1)}) %reduce-scatter.3.cloned.1.call-update) | async-done | bytes 2097168 | tf_op jit(solution)/shard_map/reduce_scatter | solution.py:35
  102.4 0.0 reduce-scatter.5.cloned.1.call-update
  102.4 85.1 %reduce-scatter.5.cloned.1.call-done = bf16[64,1024]{1,0:T(8,128)(2,1)} async-done(((bf16[1024,1024]{1,0:T(8,128)(2,1)}), bf16[64,1024]{1,0:T(8,128)(2,1)}) %reduce-scatter.5.cloned.1.call-update) | async-done | bytes 131088 | tf_op jit(solution)/shard_map/reduce_scatter | solution.py:36
  (3 shorter events, 0.1 us)
Async XLA Ops:
  6.5 75.0 %copy-start = (bf16[1,512,2048]{2,1,0:T(8,128)(2,1)S(1)}, bf16[1,512,2048]{2,1,0:T(8,128)(2,1)}, u32[]{:S(2)}) copy-start(bf16[1,512,2048]{2,1,0:T(8,128)(2,1)} %param.12) | copy-start | bytes 6291460
  6.5 68.4 %all-gather.3.cloned.1.call-start = ((), (), s32[]{:S(2)}) async-start(), calls=%async_computation.2 | async-start | bytes 4325376 | tf_op jit(solution)/shard_map/all_gather | solution.py:22
  9.4 93.0 %reduce-scatter.3.cloned.1.call-start = ((), (), s32[]{:S(2)}) async-start(), calls=%async_computation.3 | async-start | bytes 6291456 | tf_op jit(solution)/shard_map/reduce_scatter | solution.py:35
  91.6 95.9 %reduce-scatter.5.cloned.1.call-start = ((), (), s32[]{:S(2)}) async-start(), calls=%async_computation.4 | async-start | bytes 2228224 | tf_op jit(solution)/shard_map/reduce_scatter | solution.py:36
Sparse Core Ops, SparseCore 0:
  10.2 64.7 all-gather.2
  91.7 10.6 reduce-scatter.2
  104.7 82.7 reduce-scatter.4
where the time goes:
time: 194 us
  waiting for transfers between devices  115 us (59%)
  blocking collectives  43.3 us (22%)
  matrix products  16.6 us (9%)
  between operations  13.1 us (7%)
  other arithmetic  5.67 us (3%)
    reduce_scatter x1, waiting for transfers between devices, on_device(): return lax.psum_scatter(halves, 'ep', scatter_dimension=0, tiled=True)  85.1 us
    all_gather x1, blocking collectives, on_device(): all_gates = lax.all_gather(gates, 'ep', axis=0, tiled=True)  43.3 us
    all_gather x1, waiting for transfers between devices, on_device(): rows = lax.all_gather(normed, ('ep', 'tp'), axis=0, tiled=True)  19.2 us
    reduce_scatter x1, waiting for transfers between devices, on_device(): halves = lax.psum_scatter(weighted, 'tp', scatter_dimension=1, tiled=True)  10.8 us
    dot_general x1, matrix products, on_device(): jnp.dot(hidden, down_proj[0], preferred_element_type=jnp.float32)  10.1 us
    dot_general x1, matrix products, on_device(): up_acts = jnp.dot(rows, up_proj[0], preferred_element_type=jnp.float32)  6.59 us
  transfers between devices with their start and end apart: 3, of which 3 were waited for; matrix products, arithmetic and copies ran while one was open for 2% of the time, Pallas kernels for 0%

commit v1 on v0

--- a/solution.py
+++ b/solution.py
@@ -25,7 +25,13 @@
     named = route_ids[:, :, None] == experts[None, None, :]
     chosen = jnp.sum(jnp.where(named, share_of[:, :, None], 0.0), axis=1)
     gates = chosen * jnp.repeat(group_weight, EXP_GRP, axis=1)
-    all_gates = lax.all_gather(gates, "ep", axis=0, tiled=True)
+    size = lax.axis_size("ep")
+    held, blocks = (gates, [gates])
+    for _ in range(size - 1):
+        held = lax.ppermute(held, "ep", [(i, (i + 1) % size) for i in range(size)])
+        blocks.insert(0, held)
+    line = jnp.concatenate(blocks, axis=0)
+    all_gates = jnp.roll(line, (lax.axis_index("ep") + 1) * gates.shape[0], axis=0)
     own_gate = lax.dynamic_slice_in_dim(all_gates, lax.axis_index("ep"), 1, 1)
     gate_acts = jnp.dot(rows, gate_proj[0], preferred_element_type=jnp.float32)
     up_acts = jnp.dot(rows, up_proj[0], preferred_element_type=jnp.float32)

time: 194 us -> 240 us (1.24)
  waiting for transfers between devices: 115 us -> 201 us
  blocking collectives: 43.3 us -> 0 us
  starting transfers between devices: 0.09 us -> 3.09 us
    ppermute x0 -> x15, waiting for transfers between devices: none -> 108 us  [on_device(): held = lax.ppermute(held, 'ep', [(i, (i + 1) % size) for i in range(size)])]
    all_gather x1 -> x0, blocking collectives: 43.3 us -> none  [on_device(): all_gates = lax.all_gather(gates, 'ep', axis=0, tiled=True)]
    all_gather x1, waiting for transfers between devices: 19.2 us -> 0.01 us  [on_device(): rows = lax.all_gather(normed, ('ep', 'tp'), axis=0, tiled=True)]
    ppermute x0 -> x15, starting transfers between devices: none -> 3 us  [on_device(): held = lax.ppermute(held, 'ep', [(i, (i + 1) % size) for i in range(size)])]
    reduce_scatter x1, waiting for transfers between devices: 10.8 us -> 7.84 us  [on_device(): halves = lax.psum_scatter(weighted, 'tp', scatter_dimension=1, tiled=True)]
  transfers between devices with their start and end apart: 3 -> 18, of which waited for: 3 -> 17; matrix products, arithmetic and copies ran while one was open for 2% -> 1% of each run, Pallas kernels for 0% -> 0%
where the time goes in v1:
time: 240 us; the launch traced here: 239 us
  waiting for transfers between devices  201 us (84%)
  matrix products  16.6 us (7%)
  between operations  13.1 us (5%)
  other arithmetic  5.67 us (2%)
  starting transfers between devices  3.09 us (1%)
    ppermute x15, waiting for transfers between devices, on_device(): held = lax.ppermute(held, 'ep', [(i, (i + 1) % size) for i in range(size)])  108 us
    reduce_scatter x1, waiting for transfers between devices, on_device(): return lax.psum_scatter(halves, 'ep', scatter_dimension=0, tiled=True)  85.1 us
    dot_general x1, matrix products, on_device(): jnp.dot(hidden, down_proj[0], preferred_element_type=jnp.float32)  10.1 us
    reduce_scatter x1, waiting for transfers between devices, on_device(): halves = lax.psum_scatter(weighted, 'tp', scatter_dimension=1, tiled=True)  7.84 us
    dot_general x1, matrix products, on_device(): up_acts = jnp.dot(rows, up_proj[0], preferred_element_type=jnp.float32)  6.55 us
  transfers between devices with their start and end apart: 18, of which 17 were waited for; matrix products, arithmetic and copies ran while one was open for 1% of the time, Pallas kernels for 0%

profile of v1, /device:TPU:0, one launch (start us, length us, event | category | flops | bytes accessed | tf_op | source)
XLA Modules:
  0.0 239.3 jit_solution(3165049475335349477)
XLA Ops:
  6.5 0.0 copy-start
  6.5 0.0 all-gather.2.cloned.1.call-start
  6.5 1.2 fusion.12
  7.7 1.7 fusion.14
  9.4 0.0 all-gather.2.cloned.1.call-update
  9.4 0.0 reduce-scatter.3.cloned.1.call-start
  9.5 0.7 reduce_sum.28
  10.2 0.7 broadcast_divide_fusion
  10.9 0.7 select_reduce_fusion
  11.6 0.7 bitcast_multiply_fusion
  12.3 3.0 %collective-permute-start = (f32[64,16]{0,1:T(8,128)S(1)}, f32[64,16]{0,1:T(8,128)S(1)}, u32[]{:S(2)}, u32[]{:S(2)}) collective-permute-start(f32[64,16]{0,1:T(8,128)S(1)} %bitcast_multiply_fusion), channel_id=1, source_target_pairs={{0,2},{2,4},{4,6},{6,8},{8,10},{10,12},{12,14},{14,16},{16,18},{18... | collective-permute-start | bytes 12296 | tf_op jit(solution)/shard_map/ppermute | solution.py:31
  15.3 5.6 %collective-permute-done = f32[64,16]{0,1:T(8,128)S(1)} collective-permute-done((f32[64,16]{0,1:T(8,128)S(1)}, f32[64,16]{0,1:T(8,128)S(1)}, u32[]{:S(2)}, u32[]{:S(2)}) %collective-permute-start) | collective-permute-done | bytes 4128 | tf_op jit(solution)/shard_map/ppermute | solution.py:31
  20.9 0.0 collective-permute-start.1
  20.9 7.3 %collective-permute-done.1 = f32[64,16]{0,1:T(8,128)S(1)} collective-permute-done((f32[64,16]{0,1:T(8,128)S(1)}, f32[64,16]{0,1:T(8,128)S(1)}, u32[]{:S(2)}, u32[]{:S(2)}) %collective-permute-start.1) | collective-permute-done | bytes 4128 | tf_op jit(solution)/shard_map/ppermute | solution.py:31
  28.1 0.0 collective-permute-start.2
  28.1 7.3 %collective-permute-done.2 = f32[64,16]{0,1:T(8,128)S(1)} collective-permute-done((f32[64,16]{0,1:T(8,128)S(1)}, f32[64,16]{0,1:T(8,128)S(1)}, u32[]{:S(2)}, u32[]{:S(2)}) %collective-permute-start.2) | collective-permute-done | bytes 4128 | tf_op jit(solution)/shard_map/ppermute | solution.py:31
  35.4 0.0 collective-permute-start.3
  35.5 7.4 %collective-permute-done.3 = f32[64,16]{0,1:T(8,128)S(1)} collective-permute-done((f32[64,16]{0,1:T(8,128)S(1)}, f32[64,16]{0,1:T(8,128)S(1)}, u32[]{:S(2)}, u32[]{:S(2)}) %collective-permute-start.3) | collective-permute-done | bytes 4128 | tf_op jit(solution)/shard_map/ppermute | solution.py:31
  42.8 0.0 collective-permute-start.4
  42.8 7.2 %collective-permute-done.4 = f32[64,16]{0,1:T(8,128)S(1)} collective-permute-done((f32[64,16]{0,1:T(8,128)S(1)}, f32[64,16]{0,1:T(8,128)S(1)}, u32[]{:S(2)}, u32[]{:S(2)}) %collective-permute-start.4) | collective-permute-done | bytes 4128 | tf_op jit(solution)/shard_map/ppermute | solution.py:31
  50.1 0.0 collective-permute-start.5
  50.1 7.2 %collective-permute-done.5 = f32[64,16]{0,1:T(8,128)S(1)} collective-permute-done((f32[64,16]{0,1:T(8,128)S(1)}, f32[64,16]{0,1:T(8,128)S(1)}, u32[]{:S(2)}, u32[]{:S(2)}) %collective-permute-start.5) | collective-permute-done | bytes 4128 | tf_op jit(solution)/shard_map/ppermute | solution.py:31
  57.3 0.0 collective-permute-start.6
  57.3 7.5 %collective-permute-done.6 = f32[64,16]{0,1:T(8,128)S(1)} collective-permute-done((f32[64,16]{0,1:T(8,128)S(1)}, f32[64,16]{0,1:T(8,128)S(1)}, u32[]{:S(2)}, u32[]{:S(2)}) %collective-permute-start.6) | collective-permute-done | bytes 4128 | tf_op jit(solution)/shard_map/ppermute | solution.py:31
  64.9 0.0 collective-permute-start.7
  64.9 7.3 %collective-permute-done.7 = f32[64,16]{0,1:T(8,128)S(1)} collective-permute-done((f32[64,16]{0,1:T(8,128)S(1)}, f32[64,16]{0,1:T(8,128)S(1)}, u32[]{:S(2)}, u32[]{:S(2)}) %collective-permute-start.7) | collective-permute-done | bytes 4128 | tf_op jit(solution)/shard_map/ppermute | solution.py:31
  72.1 0.0 collective-permute-start.8
  72.1 7.2 %collective-permute-done.8 = f32[64,16]{0,1:T(8,128)S(1)} collective-permute-done((f32[64,16]{0,1:T(8,128)S(1)}, f32[64,16]{0,1:T(8,128)S(1)}, u32[]{:S(2)}, u32[]{:S(2)}) %collective-permute-start.8) | collective-permute-done | bytes 4128 | tf_op jit(solution)/shard_map/ppermute | solution.py:31
  79.4 0.0 collective-permute-start.9
  79.4 7.2 %collective-permute-done.9 = f32[64,16]{0,1:T(8,128)S(1)} collective-permute-done((f32[64,16]{0,1:T(8,128)S(1)}, f32[64,16]{0,1:T(8,128)S(1)}, u32[]{:S(2)}, u32[]{:S(2)}) %collective-permute-start.9) | collective-permute-done | bytes 4128 | tf_op jit(solution)/shard_map/ppermute | solution.py:31
  86.6 0.0 collective-permute-start.10
  86.6 7.2 %collective-permute-done.10 = f32[64,16]{0,1:T(8,128)S(1)} collective-permute-done((f32[64,16]{0,1:T(8,128)S(1)}, f32[64,16]{0,1:T(8,128)S(1)}, u32[]{:S(2)}, u32[]{:S(2)}) %collective-permute-start.10) | collective-permute-done | bytes 4128 | tf_op jit(solution)/shard_map/ppermute | solution.py:31
  93.9 0.0 collective-permute-start.11
  93.9 7.2 %collective-permute-done.11 = f32[64,16]{0,1:T(8,128)S(1)} collective-permute-done((f32[64,16]{0,1:T(8,128)S(1)}, f32[64,16]{0,1:T(8,128)S(1)}, u32[]{:S(2)}, u32[]{:S(2)}) %collective-permute-start.11) | collective-permute-done | bytes 4128 | tf_op jit(solution)/shard_map/ppermute | solution.py:31
  101.1 0.0 collective-permute-start.12
  101.1 7.2 %collective-permute-done.12 = f32[64,16]{0,1:T(8,128)S(1)} collective-permute-done((f32[64,16]{0,1:T(8,128)S(1)}, f32[64,16]{0,1:T(8,128)S(1)}, u32[]{:S(2)}, u32[]{:S(2)}) %collective-permute-start.12) | collective-permute-done | bytes 4128 | tf_op jit(solution)/shard_map/ppermute | solution.py:31
  108.4 0.0 collective-permute-start.13
  108.4 7.2 %collective-permute-done.13 = f32[64,16]{0,1:T(8,128)S(1)} collective-permute-done((f32[64,16]{0,1:T(8,128)S(1)}, f32[64,16]{0,1:T(8,128)S(1)}, u32[]{:S(2)}, u32[]{:S(2)}) %collective-permute-start.13) | collective-permute-done | bytes 4128 | tf_op jit(solution)/shard_map/ppermute | solution.py:31
  115.6 0.0 collective-permute-start.14
  115.6 7.2 %collective-permute-done.14 = f32[64,16]{0,1:T(8,128)S(1)} collective-permute-done((f32[64,16]{0,1:T(8,128)S(1)}, f32[64,16]{0,1:T(8,128)S(1)}, u32[]{:S(2)}, u32[]{:S(2)}) %collective-permute-start.14) | collective-permute-done | bytes 4128 | tf_op jit(solution)/shard_map/ppermute | solution.py:31
  122.9 0.1 concatenate.6
  123.0 0.1 dynamic_slice.9
  123.1 0.0 all-gather.2.cloned.1.call-done
  123.1 6.5 %fusion.4 = f32[1024,512]{1,0:T(8,128)} fusion(bf16[1024,2048]{1,0:T(8,128)(2,1)} %all-gather.2.cloned.1.call-done, bf16[1,2048,512]{2,1,0:T(8,128)(2,1)} %param.11), kind=kOutput, calls=%fused_computation.3 | convolution fusion | flops 2147483648 | bytes 8388608 | tf_op jit(solution)/shard_map/dot_general | solution.py:37
  129.6 0.0 copy-done
  129.6 10.1 %multiply_convert_fusion = bf16[1024,2048]{1,0:T(8,128)(2,1)} fusion(f32[1024]{0:T(1024)S(1)} %bitcast.20, bf16[1,512,2048]{2,1,0:T(8,128)(2,1)S(1)} %copy-done, f32[1024,512]{1,0:T(8,128)} %fusion.4, bf16[1024,2048]{1,0:T(8,128)(2,1)} %all-gather.2.cloned.1.call-done, bf16[1,2048,512]{2,1,0:T(8,128)(2,1)} %param.10), kind=kOutput, calls=%fused_computation | convolution fusion | flops 4302307328 | bytes 14684160 | tf_op jit(solution)/shard_map/dot_general | solution.py:39
  139.7 0.0 reduce-scatter.3.cloned.1.call-update
  139.7 0.0 reduce-scatter.5.cloned.1.call-start
  139.8 7.8 %reduce-scatter.3.cloned.1.call-done = bf16[1024,1024]{1,0:T(8,128)(2,1)} async-done(((bf16[1024,2048]{1,0:T(8,128)(2,1)}), bf16[1024,1024]{1,0:T(8,128)(2,1)}) %reduce-scatter.3.cloned.1.call-update) | async-done | bytes 2097168 | tf_op jit(solution)/shard_map/reduce_scatter | solution.py:41
  147.6 0.0 reduce-scatter.5.cloned.1.call-update
  147.6 85.1 %reduce-scatter.5.cloned.1.call-done = bf16[64,1024]{1,0:T(8,128)(2,1)} async-done(((bf16[1024,1024]{1,0:T(8,128)(2,1)}), bf16[64,1024]{1,0:T(8,128)(2,1)}) %reduce-scatter.5.cloned.1.call-update) | async-done | bytes 131088 | tf_op jit(solution)/shard_map/reduce_scatter | solution.py:42
  (1 shorter events, 0.0 us)
Async XLA Ops:
  6.5 123.1 %copy-start = (bf16[1,512,2048]{2,1,0:T(8,128)(2,1)S(1)}, bf16[1,512,2048]{2,1,0:T(8,128)(2,1)}, u32[]{:S(2)}) copy-start(bf16[1,512,2048]{2,1,0:T(8,128)(2,1)} %param.12) | copy-start | bytes 6291460
  6.5 116.5 %all-gather.2.cloned.1.call-start = ((), (), s32[]{:S(2)}) async-start(), calls=%async_computation.2 | async-start | bytes 4325376 | tf_op jit(solution)/shard_map/all_gather | solution.py:22
  9.4 138.2 %reduce-scatter.3.cloned.1.call-start = ((), (), s32[]{:S(2)}) async-start(), calls=%async_computation.3 | async-start | bytes 6291456 | tf_op jit(solution)/shard_map/reduce_scatter | solution.py:41
  12.3 8.6 %collective-permute-start = (f32[64,16]{0,1:T(8,128)S(1)}, f32[64,16]{0,1:T(8,128)S(1)}, u32[]{:S(2)}, u32[]{:S(2)}) collective-permute-start(f32[64,16]{0,1:T(8,128)S(1)} %bitcast_multiply_fusion), channel_id=1, source_target_pairs={{0,2},{2,4},{4,6},{6,8},{8,10},{10,12},{12,14},{14,16},{16,18},{18... | collective-permute-start | bytes 12296 | tf_op jit(solution)/shard_map/ppermute | solution.py:31
  20.9 7.3 %collective-permute-start.1 = (f32[64,16]{0,1:T(8,128)S(1)}, f32[64,16]{0,1:T(8,128)S(1)}, u32[]{:S(2)}, u32[]{:S(2)}) collective-permute-start(f32[64,16]{0,1:T(8,128)S(1)} %collective-permute-done), channel_id=1, source_target_pairs={{0,2},{2,4},{4,6},{6,8},{8,10},{10,12},{12,14},{14,16},{16,18},{18... | collective-permute-start | bytes 12296 | tf_op jit(solution)/shard_map/ppermute | solution.py:31
  28.1 7.3 %collective-permute-start.2 = (f32[64,16]{0,1:T(8,128)S(1)}, f32[64,16]{0,1:T(8,128)S(1)}, u32[]{:S(2)}, u32[]{:S(2)}) collective-permute-start(f32[64,16]{0,1:T(8,128)S(1)} %collective-permute-done.1), channel_id=1, source_target_pairs={{0,2},{2,4},{4,6},{6,8},{8,10},{10,12},{12,14},{14,16},{16,18},{18... | collective-permute-start | bytes 12296 | tf_op jit(solution)/shard_map/ppermute | solution.py:31
  35.4 7.4 %collective-permute-start.3 = (f32[64,16]{0,1:T(8,128)S(1)}, f32[64,16]{0,1:T(8,128)S(1)}, u32[]{:S(2)}, u32[]{:S(2)}) collective-permute-start(f32[64,16]{0,1:T(8,128)S(1)} %collective-permute-done.2), channel_id=1, source_target_pairs={{0,2},{2,4},{4,6},{6,8},{8,10},{10,12},{12,14},{14,16},{16,18},{18... | collective-permute-start | bytes 12296 | tf_op jit(solution)/shard_map/ppermute | solution.py:31
  42.8 7.3 %collective-permute-start.4 = (f32[64,16]{0,1:T(8,128)S(1)}, f32[64,16]{0,1:T(8,128)S(1)}, u32[]{:S(2)}, u32[]{:S(2)}) collective-permute-start(f32[64,16]{0,1:T(8,128)S(1)} %collective-permute-done.3), channel_id=1, source_target_pairs={{0,2},{2,4},{4,6},{6,8},{8,10},{10,12},{12,14},{14,16},{16,18},{18... | collective-permute-start | bytes 12296 | tf_op jit(solution)/shard_map/ppermute | solution.py:31
  50.1 7.2 %collective-permute-start.5 = (f32[64,16]{0,1:T(8,128)S(1)}, f32[64,16]{0,1:T(8,128)S(1)}, u32[]{:S(2)}, u32[]{:S(2)}) collective-permute-start(f32[64,16]{0,1:T(8,128)S(1)} %collective-permute-done.4), channel_id=1, source_target_pairs={{0,2},{2,4},{4,6},{6,8},{8,10},{10,12},{12,14},{14,16},{16,18},{18... | collective-permute-start | bytes 12296 | tf_op jit(solution)/shard_map/ppermute | solution.py:31
  57.3 7.5 %collective-permute-start.6 = (f32[64,16]{0,1:T(8,128)S(1)}, f32[64,16]{0,1:T(8,128)S(1)}, u32[]{:S(2)}, u32[]{:S(2)}) collective-permute-start(f32[64,16]{0,1:T(8,128)S(1)} %collective-permute-done.5), channel_id=1, source_target_pairs={{0,2},{2,4},{4,6},{6,8},{8,10},{10,12},{12,14},{14,16},{16,18},{18... | collective-permute-start | bytes 12296 | tf_op jit(solution)/shard_map/ppermute | solution.py:31
  64.9 7.3 %collective-permute-start.7 = (f32[64,16]{0,1:T(8,128)S(1)}, f32[64,16]{0,1:T(8,128)S(1)}, u32[]{:S(2)}, u32[]{:S(2)}) collective-permute-start(f32[64,16]{0,1:T(8,128)S(1)} %collective-permute-done.6), channel_id=1, source_target_pairs={{0,2},{2,4},{4,6},{6,8},{8,10},{10,12},{12,14},{14,16},{16,18},{18... | collective-permute-start | bytes 12296 | tf_op jit(solution)/shard_map/ppermute | solution.py:31
  72.1 7.2 %collective-permute-start.8 = (f32[64,16]{0,1:T(8,128)S(1)}, f32[64,16]{0,1:T(8,128)S(1)}, u32[]{:S(2)}, u32[]{:S(2)}) collective-permute-start(f32[64,16]{0,1:T(8,128)S(1)} %collective-permute-done.7), channel_id=1, source_target_pairs={{0,2},{2,4},{4,6},{6,8},{8,10},{10,12},{12,14},{14,16},{16,18},{18... | collective-permute-start | bytes 12296 | tf_op jit(solution)/shard_map/ppermute | solution.py:31
  79.4 7.2 %collective-permute-start.9 = (f32[64,16]{0,1:T(8,128)S(1)}, f32[64,16]{0,1:T(8,128)S(1)}, u32[]{:S(2)}, u32[]{:S(2)}) collective-permute-start(f32[64,16]{0,1:T(8,128)S(1)} %collective-permute-done.8), channel_id=1, source_target_pairs={{0,2},{2,4},{4,6},{6,8},{8,10},{10,12},{12,14},{14,16},{16,18},{18... | collective-permute-start | bytes 12296 | tf_op jit(solution)/shard_map/ppermute | solution.py:31
  86.6 7.2 %collective-permute-start.10 = (f32[64,16]{0,1:T(8,128)S(1)}, f32[64,16]{0,1:T(8,128)S(1)}, u32[]{:S(2)}, u32[]{:S(2)}) collective-permute-start(f32[64,16]{0,1:T(8,128)S(1)} %collective-permute-done.9), channel_id=1, source_target_pairs={{0,2},{2,4},{4,6},{6,8},{8,10},{10,12},{12,14},{14,16},{16,18},{18... | collective-permute-start | bytes 12296 | tf_op jit(solution)/shard_map/ppermute | solution.py:31
  93.9 7.2 %collective-permute-start.11 = (f32[64,16]{0,1:T(8,128)S(1)}, f32[64,16]{0,1:T(8,128)S(1)}, u32[]{:S(2)}, u32[]{:S(2)}) collective-permute-start(f32[64,16]{0,1:T(8,128)S(1)} %collective-permute-done.10), channel_id=1, source_target_pairs={{0,2},{2,4},{4,6},{6,8},{8,10},{10,12},{12,14},{14,16},{16,18},{18... | collective-permute-start | bytes 12296 | tf_op jit(solution)/shard_map/ppermute | solution.py:31
  101.1 7.2 %collective-permute-start.12 = (f32[64,16]{0,1:T(8,128)S(1)}, f32[64,16]{0,1:T(8,128)S(1)}, u32[]{:S(2)}, u32[]{:S(2)}) collective-permute-start(f32[64,16]{0,1:T(8,128)S(1)} %collective-permute-done.11), channel_id=1, source_target_pairs={{0,2},{2,4},{4,6},{6,8},{8,10},{10,12},{12,14},{14,16},{16,18},{18... | collective-permute-start | bytes 12296 | tf_op jit(solution)/shard_map/ppermute | solution.py:31
  108.4 7.2 %collective-permute-start.13 = (f32[64,16]{0,1:T(8,128)S(1)}, f32[64,16]{0,1:T(8,128)S(1)}, u32[]{:S(2)}, u32[]{:S(2)}) collective-permute-start(f32[64,16]{0,1:T(8,128)S(1)} %collective-permute-done.12), channel_id=1, source_target_pairs={{0,2},{2,4},{4,6},{6,8},{8,10},{10,12},{12,14},{14,16},{16,18},{18... | collective-permute-start | bytes 12296 | tf_op jit(solution)/shard_map/ppermute | solution.py:31
  115.6 7.2 %collective-permute-start.14 = (f32[64,16]{0,1:T(8,128)S(1)}, f32[64,16]{0,1:T(8,128)S(1)}, u32[]{:S(2)}, u32[]{:S(2)}) collective-permute-start(f32[64,16]{0,1:T(8,128)S(1)} %collective-permute-done.13), channel_id=1, source_target_pairs={{0,2},{2,4},{4,6},{6,8},{8,10},{10,12},{12,14},{14,16},{16,18},{18... | collective-permute-start | bytes 12296 | tf_op jit(solution)/shard_map/ppermute | solution.py:31
  139.7 93.0 %reduce-scatter.5.cloned.1.call-start = ((), (), s32[]{:S(2)}) async-start(), calls=%async_computation.4 | async-start | bytes 2228224 | tf_op jit(solution)/shard_map/reduce_scatter | solution.py:42
Sparse Core Ops, SparseCore 0:
  10.2 64.7 all-gather.1
  139.9 7.7 reduce-scatter.2
  149.9 82.8 reduce-scatter.4
